TPU v7x, 32 devices: a whole 2x2x4 slice. The times are simulated.
32 devices in a mesh: grp: 2 (over y), sp: 4 (over z), tp: 4 (over x, core).
Axes of the slice: x: 2, y: 2, z: 4, core: 2. Of those that a mesh axis runs over, the one named last changes fastest.
Arguments:
- tokens: bfloat16 [3072, 2048], P(('grp', 'sp'), 'tp'), parts along dimension 0, may hold values from -6 to 6
- norm_gain: float32 [2048], replicated, may hold values from 0.1 to 1.9
- qk_gain: float32 [4, 64], replicated, may hold values from 0.7 to 5.5
- w_query_window: bfloat16 [2048, 1024], P('sp', 'tp'), may hold values from -1 to 1
- w_key_window: bfloat16 [2048, 512], P('sp', 'tp'), may hold values from -1 to 1
- w_value_window: bfloat16 [2048, 512], P('sp', 'tp'), may hold values from -0.125 to 0.125
- sink_logits: float32 [16], P('tp'), may hold values from 0 to 5
- w_query_forget: bfloat16 [2048, 1024], P('sp', 'tp'), may hold values from -1 to 1
- w_key_forget: bfloat16 [2048, 1024], P('sp', 'tp'), may hold values from -1 to 1
- w_value_forget: bfloat16 [2048, 1024], P('sp', 'tp'), may hold values from -0.125 to 0.125
- gate_cum: float32 [3072, 16], P(('grp', 'sp'), 'tp'), parts along dimension 0, as said below
- w_merge: bfloat16 [2048, 2, 2048], P('sp', None, 'tp'), may hold values from -0.125 to 0.125
- w_branch: bfloat16 [2, 1024, 2048], P(None, 'sp', 'tp'), may hold values from -0.8984375 to 0.8984375
Outputs:
- mixed: bfloat16 [3072, 2048], P(('grp', 'sp'), 'tp'), parts along dimension 0
There are 2 independent parts, one for each index of `grp`. A program takes and returns all parts, laid end to end along the dimension named above; an argument that names none is the same for every part. Nothing has to cross between parts.
Inputs may be any that keep to these rules, and one draw needn't show every extreme that they name: `gate_cum`: along positions each head's values never rise.
All inputs are finite; a program needn't handle non-finite values.
Results may differ from a plain program's by a relative error of at most 0.012.
Values may be sent and summed in bfloat16 or wider, within the bound.
A program may use at most 64 MiB of HBM per device.

v0:
```python
import math
import jax
import jax.numpy as jnp
from jax import lax
from jax.sharding import PartitionSpec as P

HEAD = 64
WINDOW = 128
epsilon = 1e-06
big_negative = -1e30


def from_behind(value, axis, by):
    size = lax.axis_size(axis)
    pairs = [(i, i + by) for i in range(size) if 0 <= i + by < size]
    return lax.ppermute(value, axis, pairs)


def head_norm(raw, gain, head_count):
    split = raw.reshape(raw.shape[0], head_count, -1)
    scaled = split * lax.rsqrt(jnp.mean(split * split, axis=-1, keepdims=True) + epsilon) * gain
    return scaled.astype(jnp.bfloat16)


def window_attend(queries, keys_ext, values_ext, sink_rows, first_pos):
    row_count, head_count, head_size = queries.shape
    group_count = keys_ext.shape[1]
    span_rows = WINDOW // 2
    block_count = row_count // span_rows
    query_blocks = queries.reshape(
        block_count, span_rows, group_count, head_count // group_count, head_size
    )
    key_blocks = jnp.concatenate(
        [
            keys_ext[lag_index * span_rows : lag_index * span_rows + row_count].reshape(
                block_count, span_rows, group_count, head_size
            )
            for lag_index in range(3)
        ],
        axis=1,
    )
    value_blocks = jnp.concatenate(
        [
            values_ext[lag_index * span_rows : lag_index * span_rows + row_count].reshape(
                block_count, span_rows, group_count, head_size
            )
            for lag_index in range(3)
        ],
        axis=1,
    )
    scores = jnp.einsum(
        "nqgrd,nkgd->ngrqk", query_blocks, key_blocks, preferred_element_type=jnp.float32
    ) * head_size ** (-0.5)
    distance = WINDOW + jnp.arange(span_rows)[:, None] - jnp.arange(3 * span_rows)[None, :]
    key_pos = (
        first_pos
        - WINDOW
        + jnp.arange(block_count)[:, None] * span_rows
        + jnp.arange(3 * span_rows)[None, :]
    )
    is_valid = ((distance >= 0) & (distance < WINDOW))[None] & (key_pos >= 0)[:, None, :]
    is_valid = is_valid[:, None, None]
    sink_grid = sink_rows.reshape(1, group_count, head_count // group_count, 1)
    row_max = jnp.maximum(jnp.max(jnp.where(is_valid, scores, big_negative), axis=-1), sink_grid)
    weights = jnp.where(is_valid, jnp.exp(scores - row_max[..., None]), 0.0)
    row_total = jnp.sum(weights, axis=-1) + jnp.exp(sink_grid - row_max)
    prob_rows = (weights / row_total[..., None]).astype(jnp.bfloat16)
    mixed_sum = jnp.einsum(
        "ngrqk,nkgd->nqgrd", prob_rows, value_blocks, preferred_element_type=jnp.float32
    )
    return mixed_sum.reshape(row_count, head_count * head_size).astype(jnp.bfloat16)


def forget_groups(groups, keys, values, gates):
    head_count, head_size = (keys.shape[1], keys.shape[2])
    gates_all = lax.all_gather(gates, "sp", axis=0, tiled=True)

    def absorber(queries, query_gate, query_pos):

        def absorb(running, block):
            row_max, row_total, mixed_sum = running
            key_rows, value_rows, key_gate, key_pos = block
            scores = jnp.einsum(
                "qhd,khd->hqk", queries, key_rows, preferred_element_type=jnp.float32
            ) * head_size ** (-0.5)
            scores = scores + query_gate.T[:, :, None] - key_gate.T[:, None, :]
            is_valid = (query_pos[:, None] >= key_pos[None, :])[None]
            new_max = jnp.maximum(
                row_max, jnp.max(jnp.where(is_valid, scores, big_negative), axis=-1)
            )
            weights = jnp.where(is_valid, jnp.exp(scores - new_max[..., None]), 0.0)
            shrink = jnp.exp(row_max - new_max)
            row_total = row_total * shrink + jnp.sum(weights, axis=-1)
            mixed_sum = mixed_sum * shrink.T[:, :, None] + jnp.einsum(
                "hqk,khd->qhd",
                weights.astype(jnp.bfloat16),
                value_rows,
                preferred_element_type=jnp.float32,
            )
            return ((new_max, row_total, mixed_sum), None)

        return absorb

    initial = tuple(
        (
            (
                jnp.full((head_count, group[0].shape[0]), big_negative, jnp.float32),
                jnp.zeros((head_count, group[0].shape[0]), jnp.float32),
                jnp.zeros((group[0].shape[0], head_count, head_size), jnp.float32),
            )
            for group in groups
        )
    )
    first_row = jnp.int32(0)
    key_rows = lax.all_gather(keys, "sp", axis=0, tiled=True)
    value_rows = lax.all_gather(values, "sp", axis=0, tiled=True)
    piece_rows = key_rows.shape[0]
    sub_rows = math.gcd(piece_rows, 2048)
    turns = piece_rows // sub_rows
    key_gate = gates_all
    key_pos = jnp.arange(piece_rows)
    blocks = (
        key_rows.reshape(turns, sub_rows, head_count, head_size),
        value_rows.reshape(turns, sub_rows, head_count, head_size),
        key_gate.reshape(turns, sub_rows, head_count),
        key_pos.reshape(turns, sub_rows),
    )
    updated = []
    for (queries, query_gate, query_pos), state in zip(groups, initial):
        absorb = absorber(queries, query_gate, query_pos)

        def advance(current):
            return lax.scan(absorb, current, blocks)[0]

        def keep(current):
            return current

        updated.append(lax.cond(first_row <= query_pos[-1], advance, keep, state))
    finals = tuple(updated)
    return [
        (mixed_sum / row_total.T[:, :, None])
        .reshape(mixed_sum.shape[0], head_count * head_size)
        .astype(jnp.bfloat16)
        for row_max, row_total, mixed_sum in finals
    ]


def on_device(
    tokens,
    norm_gain,
    qk_gain,
    w_query_window,
    w_key_window,
    w_value_window,
    sink_logits,
    w_query_forget,
    w_key_forget,
    w_value_forget,
    gate_cum,
    w_merge,
    w_branch,
):
    row_count = tokens.shape[0]
    row_offset = lax.axis_index("sp") * row_count
    gathered = lax.all_gather(tokens, "tp", axis=1, tiled=True)
    as_float = gathered.astype(jnp.float32)
    normed = (
        as_float
        * lax.rsqrt(jnp.mean(as_float * as_float, axis=-1, keepdims=True) + epsilon)
        * norm_gain
    ).astype(jnp.bfloat16)
    merge_flat = w_merge.reshape(w_merge.shape[0], -1)
    pieces = (
        lax.all_gather(w_query_window, "sp", axis=0, tiled=True),
        lax.all_gather(w_key_window, "sp", axis=0, tiled=True),
        lax.all_gather(w_value_window, "sp", axis=0, tiled=True),
        lax.all_gather(w_query_forget, "sp", axis=0, tiled=True),
        lax.all_gather(w_key_forget, "sp", axis=0, tiled=True),
        lax.all_gather(w_value_forget, "sp", axis=0, tiled=True),
        lax.all_gather(merge_flat, "sp", axis=0, tiled=True),
    )
    projected = tuple(
        (jnp.dot(normed, weight_rows, preferred_element_type=jnp.float32) for weight_rows in pieces)
    )
    query_heads = w_query_window.shape[1] // HEAD
    group_heads = w_key_window.shape[1] // HEAD
    window_query = head_norm(projected[0], qk_gain[0], query_heads)
    window_key = head_norm(projected[1], qk_gain[1], group_heads)
    window_value = projected[2].astype(jnp.bfloat16).reshape(row_count, group_heads, HEAD)
    prev_key, prev_value = from_behind(
        (window_key[row_count - WINDOW :], window_value[row_count - WINDOW :]), "sp", 1
    )
    window_out = window_attend(
        window_query,
        jnp.concatenate([prev_key, window_key], axis=0),
        jnp.concatenate([prev_value, window_value], axis=0),
        sink_logits,
        row_offset,
    )
    forget_query = head_norm(projected[3], qk_gain[2], query_heads)
    forget_key = head_norm(projected[4], qk_gain[3], query_heads)
    forget_value = projected[5].astype(jnp.bfloat16).reshape(row_count, query_heads, HEAD)
    own_pos = row_offset + jnp.arange(row_count)
    forget_out = forget_groups(
        [(forget_query, gate_cum, own_pos)], forget_key, forget_value, gate_cum
    )[0]
    channel_count = w_merge.shape[2]
    merge_gate = jax.nn.sigmoid(projected[6]).reshape(row_count, 2, channel_count)
    branch_full = lax.all_gather(w_branch, "sp", axis=1, tiled=True)
    head_stack = jnp.stack([window_out, forget_out], axis=1)
    weight_rows = branch_full
    projection = jnp.einsum(
        "uxa,xag->uxg",
        lax.all_gather(head_stack, "tp", axis=2, tiled=True),
        weight_rows,
        preferred_element_type=jnp.float32,
    )
    return (merge_gate[:, 0] * projection[:, 0] + merge_gate[:, 1] * projection[:, 1]).astype(
        jnp.bfloat16
    )


def solution(mesh):
    return jax.shard_map(
        on_device,
        mesh=mesh,
        in_specs=(
            P(("grp", "sp"), "tp"),
            P(),
            P(),
            P("sp", "tp"),
            P("sp", "tp"),
            P("sp", "tp"),
            P("tp"),
            P("sp", "tp"),
            P("sp", "tp"),
            P("sp", "tp"),
            P(("grp", "sp"), "tp"),
            P("sp", None, "tp"),
            P(None, "sp", "tp"),
        ),
        out_specs=P(("grp", "sp"), "tp"),
        check_vma=False,
    )
```

profile of v0, /device:TPU:0, one launch (start us, length us, event | category | flops | bytes accessed | tf_op | source)
XLA Modules:
  0.0 339.6 jit_solution(14842164746860835694)
XLA Ops:
  13.7 16.6 %all_gather.48 = f32[1536,4]{0,1:T(4,128)} all-gather(f32[384,4]{0,1:T(4,128)} %param.27), channel_id=1, replica_groups=mesh['grp'=2,'sp'=4,'tp'=4] {'sp'}, dimensions={0}, use_global_device_ids=true | all-gather | bytes 30720 | tf_op jit(solution)/shard_map/all_gather | solution.py:76
  30.5 19.0 %all_gather.42 = bf16[2048,128]{1,0:T(8,128)(2,1)} all-gather(bf16[512,128]{1,0:T(8,128)(2,1)S(1)} %copy-done.8), channel_id=1, replica_groups=mesh['grp'=2,'sp'=4,'tp'=4] {'sp'}, dimensions={0}, use_global_device_ids=true | all-gather | bytes 655360 | tf_op jit(solution)/shard_map/all_gather | solution.py:175
  50.2 21.1 %all_gather.41 = bf16[2048,128]{1,0:T(8,128)(2,1)} all-gather(bf16[512,128]{1,0:T(8,128)(2,1)S(1)} %copy-done.9), channel_id=1, replica_groups=mesh['grp'=2,'sp'=4,'tp'=4] {'sp'}, dimensions={0}, use_global_device_ids=true | all-gather | bytes 655360 | tf_op jit(solution)/shard_map/all_gather | solution.py:176
  71.9 1.9 fusion.25
  74.3 2.5 multiply_reduce_fusion.1
  77.0 25.4 %all_gather.45 = bf16[1536,4,64]{0,2,1:T(8,128)(2,1)S(1)} all-gather(bf16[384,4,64]{0,2,1:T(8,128)(2,1)S(1)} %multiply_convert_fusion.2), channel_id=1, replica_groups=mesh['grp'=2,'sp'=4,'tp'=4] {'sp'}, dimensions={0}, use_global_device_ids=true | all-gather | bytes 983040 | tf_op jit(solution)/shard_map/all_gather | solution.py:115
  102.5 5.3 %all-gather.17.cloned.1.call-done = bf16[2048,256]{1,0:T(8,128)(2,1)} async-done(((bf16[512,256]{1,0:T(8,128)(2,1)}), bf16[2048,256]{1,0:T(8,128)(2,1)}) %all-gather.17.cloned.1.call-update) | async-done | bytes 1048592 | tf_op jit(solution)/shard_map/all_gather | solution.py:179
  107.7 2.0 convolution_convert_fusion.1
  109.7 25.2 %all_gather.47 = bf16[1536,4,64]{0,2,1:T(8,128)(2,1)S(1)} all-gather(bf16[384,4,64]{0,2,1:T(8,128)(2,1)S(1)} %bitcast.165), channel_id=1, replica_groups=mesh['grp'=2,'sp'=4,'tp'=4] {'sp'}, dimensions={0}, use_global_device_ids=true | all-gather | bytes 983040 | tf_op jit(solution)/shard_map/all_gather | solution.py:116
  134.9 8.7 %all-gather.19.cloned.1.call-done = bf16[2048,256]{1,0:T(8,128)(2,1)} async-done(((bf16[512,256]{1,0:T(8,128)(2,1)}), bf16[2048,256]{1,0:T(8,128)(2,1)}) %all-gather.19.cloned.1.call-update) | async-done | bytes 1048592 | tf_op jit(solution)/shard_map/all_gather | solution.py:177
  143.7 2.1 multiply_reduce_fusion
  149.0 35.5 %conditional.1 = (f32[4,384]{1,0:T(4,128)}, f32[384,4,64]{0,2,1:T(8,128)}) conditional(s32[]{:T(128)} %bitcast.13, () %tuple.20, (bf16[1536,4,64]{0,2,1:T(8,128)(2,1)S(1)}, bf16[1536,4,64]{0,2,1:T(8,128)(2,1)S(1)}, f32[1536,4]{0,1:T(4,128)}, s32[3,512]{1,0:T(4,128)S(1)}, s32[3,512]{1,0:T(4,128)S(1)}, /*index=5*/s32[384]{0:T(512)}, ...), branch_computations={%region_7.8_spmd, %region_8.13_spmd} | conditional | flops 215199744 | bytes 15060769 | solution.py:138
  149.6 1.4 copy_bitcast_fusion
  151.0 33.5 %while.18 = (s32[]{:T(128)}, f32[4,384]{1,0:T(4,128)S(1)}, f32[4,384]{1,0:T(4,128)}, f32[384,4,64]{0,2,1:T(8,128)}, s32[384]{0:T(512)}, /*index=5*/s32[3,512]{1,...) while((s32[]{:T(128)}, f32[4,384]{1,0:T(4,128)S(1)}, ...), condition=%wide.region_12.12_spmd.clone, body=%wide.region_9.11_spmd.clone.sunk | while | flops 215196672 | bytes 11896481 | solution.py:133
  153.2 2.7 fusion.85
  156.6 1.6 fusion.87
  158.8 2.7 fusion.89
  163.8 2.7 fusion.85
  167.2 1.6 fusion.87
  170.1 2.9 fusion.89
  175.3 2.7 fusion.85
  178.7 1.6 fusion.87
  181.6 2.9 fusion.89
  185.5 2.5 bitcast_reduce_fusion
  189.8 2.8 collective-permute-start.1
  192.6 3.3 collective-permute-start
  203.8 14.9 %all-gather.23.cloned.1.call-done = bf16[2,1024,512]{2,1,0:T(8,128)(2,1)} async-done(((bf16[2,256,512]{2,1,0:T(8,128)(2,1)}), bf16[2,1024,512]{2,1,0:T(8,128)(2,1)}) %all-gather.23.cloned.1.call-update) | async-done | bytes 2097168 | tf_op jit(solution)/shard_map/all_gather | solution.py:209
  218.6 21.5 %all-gather.21.cloned.1.call-done = bf16[384,2,1024]{2,0,1:T(8,128)(2,1)} async-done(((bf16[384,2,256]{2,0,1:T(8,128)(2,1)}), bf16[384,2,1024]{2,0,1:T(8,128)(2,1)}) %all-gather.21.cloned.1.call-update) | async-done | bytes 1572880 | tf_op jit(solution)/shard_map/all_gather | solution.py:214
  240.2 3.0 convolution_bitcast_fusion
  243.2 79.3 %all-gather.11.cloned.1.call-done = bf16[2048,1024]{1,0:T(8,128)(2,1)} async-done(((bf16[512,1024]{1,0:T(8,128)(2,1)}), bf16[2048,1024]{1,0:T(8,128)(2,1)}) %all-gather.11.cloned.1.call-update) | async-done | bytes 4194320 | tf_op jit(solution)/shard_map/all_gather | solution.py:180
  322.5 5.3 %add_divide_fusion = f32[384,1024]{1,0:T(8,128)} fusion(bf16[384,2048]{1,0:T(8,128)(2,1)S(1)} %copy-done.1, bf16[2048,1024]{1,0:T(8,128)(2,1)} %all-gather.11.cloned.1.call-done), kind=kOutput, calls=%fused_computation.44 | convolution fusion | flops 1611792384 | bytes 7340032 | tf_op jit(solution)/shard_map/dot_general | solution.py:183
  327.8 2.6 reshape.258
  (135 shorter events, 37.0 us)
Async XLA Ops:
  6.5 6.6 %copy-start.15 = (f32[4,64]{1,0:T(4,128)S(1)}, f32[4,64]{1,0:T(4,128)}, u32[]{:S(2)}) copy-start(f32[4,64]{1,0:T(4,128)} %param.19) | copy-start | bytes 3076
  6.5 24.0 %copy-start.8 = (bf16[512,128]{1,0:T(8,128)(2,1)S(1)}, bf16[512,128]{1,0:T(8,128)(2,1)}, u32[]{:S(2)}) copy-start(bf16[512,128]{1,0:T(8,128)(2,1)} %param.21) | copy-start | bytes 393220
  6.5 42.9 %copy-start.16 = (f32[4]{0:T(128)S(1)}, f32[4]{0:T(128)}, u32[]{:S(2)}) copy-start(f32[4]{0:T(128)} %param.23) | copy-start | bytes 52
  6.5 43.6 %copy-start.9 = (bf16[512,128]{1,0:T(8,128)(2,1)S(1)}, bf16[512,128]{1,0:T(8,128)(2,1)}, u32[]{:S(2)}) copy-start(bf16[512,128]{1,0:T(8,128)(2,1)} %param.22) | copy-start | bytes 393220
  6.5 65.4 %all-gather.9.cloned.1.call-start = ((), (), s32[]{:S(2)}) async-start(), calls=%async_computation | async-start | bytes 1966080 | tf_op jit(solution)/shard_map/all_gather | solution.py:165
  7.3 67.1 %all-gather.15.cloned.1.call-start = ((), (), s32[]{:S(2)}) async-start(), calls=%async_computation.3 | async-start | bytes 1310720 | tf_op jit(solution)/shard_map/all_gather | solution.py:178
  8.0 99.7 %all-gather.17.cloned.1.call-start = ((), (), s32[]{:S(2)}) async-start(), calls=%async_computation.4 | async-start | bytes 1310720 | tf_op jit(solution)/shard_map/all_gather | solution.py:179
  8.8 134.9 %all-gather.19.cloned.1.call-start = ((), (), s32[]{:S(2)}) async-start(), calls=%async_computation.5 | async-start | bytes 1310720 | tf_op jit(solution)/shard_map/all_gather | solution.py:177
  9.3 176.2 %all-gather.13.cloned.1.call-start = ((), (), s32[]{:S(2)}) async-start(), calls=%async_computation.2 | async-start | bytes 1310720 | tf_op jit(solution)/shard_map/all_gather | solution.py:174
  9.9 208.7 %all-gather.23.cloned.1.call-start = ((), (), s32[]{:S(2)}) async-start(), calls=%async_computation.7 | async-start | bytes 2621440 | tf_op jit(solution)/shard_map/all_gather | solution.py:209
  10.5 63.4 %copy-start.11 = (f32[2048]{0:T(1024)S(1)}, f32[2048]{0:T(1024)}, u32[]{:S(2)}) copy-start(f32[2048]{0:T(1024)} %param.18) | copy-start | bytes 24580
  10.5 229.6 %all-gather.21.cloned.1.call-start = ((), (), s32[]{:S(2)}) async-start(), calls=%async_computation.6 | async-start | bytes 1966080 | tf_op jit(solution)/shard_map/all_gather | solution.py:214
  71.9 1.9 copy-start.2
  74.3 72.6 %copy-start = (bf16[384,2048]{1,0:T(8,128)(2,1)}, bf16[384,2048]{1,0:T(8,128)(2,1)S(1)}, u32[]{:S(2)}) copy-start(bf16[384,2048]{1,0:T(8,128)(2,1)S(1)} %fusion.27) | copy-start | bytes 4718596
  143.7 2.1 copy-start.3
  145.7 1.2 copy-start.4
  185.5 2.6 copy-start.5
  188.4 1.1 copy-start.10
  188.4 1.2 copy-start.12
  188.6 7.3 %copy-start.14 = (f32[64]{0:T(128)S(1)}, f32[64]{0:T(128)}, u32[]{:S(2)}) copy-start(f32[64]{0:T(128)} %get-tuple-element.195) | copy-start | bytes 772
  189.8 7.2 %collective-permute-start.1 = (bf16[128,2,64]{0,2,1:T(8,128)(2,1)S(1)}, bf16[128,2,64]{0,2,1:T(8,128)(2,1)S(1)}, u32[]{:S(2)}, u32[]{:S(2)}) collective-permute-start(bf16[128,2,64]{0,2,1:T(8,128)(2,1)S(1)} %slice.68), channel_id=1, source_target_pairs={{0,4},{4,8},{8,12},{1,5},{5,9},{9,13},{2,6},{6,10},{10,14},{3,7},{... | collective-permute-start | bytes 98312 | tf_op jit(solution)/shard_map/ppermute | solution.py:16
  192.6 5.4 %collective-permute-start = (bf16[128,2,64]{0,2,1:T(8,128)(2,1)S(1)}, bf16[128,2,64]{0,2,1:T(8,128)(2,1)S(1)}, u32[]{:S(2)}, u32[]{:S(2)}) collective-permute-start(bf16[128,2,64]{0,2,1:T(8,128)(2,1)S(1)} %bitcast.167), channel_id=1, source_target_pairs={{0,4},{4,8},{8,12},{1,5},{5,9},{9,13},{2,6},{6,10},{10,14},{3,7},{... | collective-permute-start | bytes 98312 | tf_op jit(solution)/shard_map/ppermute | solution.py:16
  197.3 1.2 copy-start.7
  198.5 0.7 copy-start.13
  200.9 1.5 copy-start.6
  202.4 120.1 %all-gather.11.cloned.1.call-start = ((), (), s32[]{:S(2)}) async-start(), calls=%async_computation.1 | async-start | bytes 5242880 | tf_op jit(solution)/shard_map/all_gather | solution.py:180
  203.8 118.7 %copy-start.1 = (bf16[384,2048]{1,0:T(8,128)(2,1)S(1)}, bf16[384,2048]{1,0:T(8,128)(2,1)}, u32[]{:S(2)}) copy-start(bf16[384,2048]{1,0:T(8,128)(2,1)} %copy-done) | copy-start | bytes 4718596
Sparse Core Ops, SparseCore 0:
  8.9 22.3 all-gather.8
  32.9 36.9 all-gather.14
  71.5 36.1 all-gather.16
  109.1 34.4 all-gather.18
  145.1 27.0 all-gather.12
  173.6 45.0 all-gather.22
  220.2 19.9 all-gather.20
  241.7 80.7 all-gather.10
where the time goes:
time: 341 us; the launch traced here: 340 us
  waiting for transfers between devices  134 us (39%)
  blocking collectives  107 us (31%)
  matrix products  37.9 us (11%)
  other arithmetic  23.1 us (7%)
  local copies, waits for them, and re-layouts  16.3 us (5%)
  between operations  14.7 us (4%)
  starting transfers between devices  6.38 us (2%)
    all_gather x1, waiting for transfers between devices, on_device(): lax.all_gather(merge_flat, 'sp', axis=0, tiled=True)  79.3 us
    all_gather x1, blocking collectives, forget_groups(): key_rows = lax.all_gather(keys, 'sp', axis=0, tiled=True)  25.4 us
    all_gather x1, blocking collectives, forget_groups(): value_rows = lax.all_gather(values, 'sp', axis=0, tiled=True)  25.2 us
    all_gather x1, waiting for transfers between devices, on_device(): lax.all_gather(head_stack, 'tp', axis=2, tiled=True)  21.5 us
    all_gather x1, blocking collectives, on_device(): lax.all_gather(w_value_window, 'sp', axis=0, tiled=True)  21.1 us
    all_gather x1, blocking collectives, on_device(): lax.all_gather(w_key_window, 'sp', axis=0, tiled=True)  19 us
    dot_general x7, matrix products, on_device(): jnp.dot(normed, weight_rows, preferred_element_type=jnp.float32)  16.8 us
    all_gather x1, blocking collectives, forget_groups(): gates_all = lax.all_gather(gates, 'sp', axis=0, tiled=True)  16.6 us
  transfers between devices with their start and end apart: 10, of which 6 were waited for; matrix products, arithmetic and copies ran while one was open for 20% of the time, Pallas kernels for 0%

commit v1 on v0

--- a/solution.py
+++ b/solution.py
@@ -112,8 +112,11 @@
         )
     )
     first_row = jnp.int32(0)
-    key_rows = lax.all_gather(keys, "sp", axis=0, tiled=True)
-    value_rows = lax.all_gather(values, "sp", axis=0, tiled=True)
+    key_rows, value_rows = jnp.split(
+        lax.all_gather(jnp.concatenate([keys, values], axis=1), "sp", axis=0, tiled=True),
+        [keys.shape[1]],
+        axis=1,
+    )
     piece_rows = key_rows.shape[0]
     sub_rows = math.gcd(piece_rows, 2048)
     turns = piece_rows // sub_rows

time: 341 us -> 357 us (1.047)
  waiting for transfers between devices: 134 us -> 197 us
  blocking collectives: 107 us -> 53 us
  local copies, waits for them, and re-layouts: 16.3 us -> 22 us
    all_gather x2 -> x0, blocking collectives: 50.7 us -> none  [the longest x1 25.4 us: forget_groups(): key_rows = lax.all_gather(keys, 'sp', axis=0, tiled=True)]
    all_gather x1, waiting for transfers between devices: 79.3 us -> 44.1 us  [on_device(): lax.all_gather(merge_flat, 'sp', axis=0, tiled=True)]
    all_gather x1, waiting for transfers between devices: 0.02 us -> 27.2 us  [on_device(): lax.all_gather(w_key_forget, 'sp', axis=0, tiled=True)]
    all_gather x1, waiting for transfers between devices: 14.9 us -> 36.6 us  [on_device(): branch_full = lax.all_gather(w_branch, 'sp', axis=1, tiled=True)]
    all_gather x1, waiting for transfers between devices: 5.25 us -> 26.8 us  [on_device(): lax.all_gather(w_value_forget, 'sp', axis=0, tiled=True)]
    all_gather x1, waiting for transfers between devices: 0.01 us -> 19.9 us  [on_device(): gathered = lax.all_gather(tokens, 'tp', axis=1, tiled=True)]
    all_gather x0 -> x1, waiting for transfers between devices: none -> 15.1 us  [forget_groups(): lax.all_gather(jnp.concatenate([keys, values], axis=1), 'sp', axis=0, til...]
    all_gather x1, waiting for transfers between devices: 8.71 us -> 0.01 us  [on_device(): lax.all_gather(w_query_forget, 'sp', axis=0, tiled=True)]
  transfers between devices with their start and end apart: 10 -> 11, of which waited for: 6 -> 8; matrix products, arithmetic and copies ran while one was open for 20% -> 22% of each run, Pallas kernels for 0% -> 0%
where the time goes in v1:
time: 357 us; the launch traced here: 356 us
  waiting for transfers between devices  197 us (55%)
  blocking collectives  53 us (15%)
  matrix products  37 us (10%)
  other arithmetic  24.8 us (7%)
  local copies, waits for them, and re-layouts  22 us (6%)
  between operations  14.3 us (4%)
  starting transfers between devices  7.03 us (2%)
    all_gather x1, waiting for transfers between devices, on_device(): lax.all_gather(merge_flat, 'sp', axis=0, tiled=True)  44.1 us
    all_gather x1, waiting for transfers between devices, on_device(): branch_full = lax.all_gather(w_branch, 'sp', axis=1, tiled=True)  36.6 us
    all_gather x1, waiting for transfers between devices, on_device(): lax.all_gather(w_key_forget, 'sp', axis=0, tiled=True)  27.2 us
    all_gather x1, waiting for transfers between devices, on_device(): lax.all_gather(w_value_forget, 'sp', axis=0, tiled=True)  26.8 us
    all_gather x1, waiting for transfers between devices, on_device(): lax.all_gather(head_stack, 'tp', axis=2, tiled=True)  20.2 us
    all_gather x1, blocking collectives, on_device(): lax.all_gather(w_value_window, 'sp', axis=0, tiled=True)  20 us
    all_gather x1, waiting for transfers between devices, on_device(): gathered = lax.all_gather(tokens, 'tp', axis=1, tiled=True)  19.9 us
    all_gather x1, blocking collectives, on_device(): lax.all_gather(w_key_window, 'sp', axis=0, tiled=True)  18.5 us
  transfers between devices with their start and end apart: 11, of which 8 were waited for; matrix products, arithmetic and copies ran while one was open for 22% of the time, Pallas kernels for 0%

profile of v1, /device:TPU:0, one launch (start us, length us, event | category | flops | bytes accessed | tf_op | source)
XLA Modules:
  0.0 355.5 jit_solution(10191989620739413122)
XLA Ops:
  11.4 19.9 %all-gather.10.cloned.1.call-done = bf16[384,2048]{1,0:T(8,128)(2,1)} async-done(((bf16[384,512]{1,0:T(8,128)(2,1)}), bf16[384,2048]{1,0:T(8,128)(2,1)}) %all-gather.10.cloned.1.call-update) | async-done | bytes 1572880 | tf_op jit(solution)/shard_map/all_gather | solution.py:168
  31.3 1.9 fusion.25
  33.7 27.2 %all-gather.16.cloned.1.call-done = bf16[2048,256]{1,0:T(8,128)(2,1)} async-done(((bf16[512,256]{1,0:T(8,128)(2,1)}), bf16[2048,256]{1,0:T(8,128)(2,1)}) %all-gather.16.cloned.1.call-update) | async-done | bytes 1048592 | tf_op jit(solution)/shard_map/all_gather | solution.py:181
  60.9 2.0 multiply_reduce_fusion.1
  63.0 26.8 %all-gather.18.cloned.1.call-done = bf16[2048,256]{1,0:T(8,128)(2,1)} async-done(((bf16[512,256]{1,0:T(8,128)(2,1)}), bf16[2048,256]{1,0:T(8,128)(2,1)}) %all-gather.18.cloned.1.call-update) | async-done | bytes 1048592 | tf_op jit(solution)/shard_map/all_gather | solution.py:182
  89.8 2.0 convolution_convert_fusion.1
  97.3 14.4 %all_gather.44 = f32[1536,4]{0,1:T(4,128)} all-gather(f32[384,4]{0,1:T(4,128)} %param.27), channel_id=1, replica_groups=mesh['grp'=2,'sp'=4,'tp'=4] {'sp'}, dimensions={0}, use_global_device_ids=true | all-gather | bytes 30720 | tf_op jit(solution)/shard_map/all_gather | solution.py:76
  111.8 18.5 %all_gather.39 = bf16[2048,128]{1,0:T(8,128)(2,1)S(1)} all-gather(bf16[512,128]{1,0:T(8,128)(2,1)S(1)} %copy-done.9), channel_id=1, replica_groups=mesh['grp'=2,'sp'=4,'tp'=4] {'sp'}, dimensions={0}, use_global_device_ids=true | all-gather | bytes 655360 | tf_op jit(solution)/shard_map/all_gather | solution.py:178
  130.5 20.0 %all_gather.38 = bf16[2048,128]{1,0:T(8,128)(2,1)S(1)} all-gather(bf16[512,128]{1,0:T(8,128)(2,1)S(1)} %copy-done.10), channel_id=1, replica_groups=mesh['grp'=2,'sp'=4,'tp'=4] {'sp'}, dimensions={0}, use_global_device_ids=true | all-gather | bytes 655360 | tf_op jit(solution)/shard_map/all_gather | solution.py:179
  151.2 2.8 multiply_reduce_fusion
  154.0 3.6 %all-gather.14.cloned.1.call-done = bf16[2048,256]{1,0:T(8,128)(2,1)} async-done(((bf16[512,256]{1,0:T(8,128)(2,1)}), bf16[2048,256]{1,0:T(8,128)(2,1)}) %all-gather.14.cloned.1.call-update) | async-done | bytes 1048592 | tf_op jit(solution)/shard_map/all_gather | solution.py:177
  157.6 2.0 bitcast_reduce_fusion
  167.1 3.5 collective-permute-start.1
  171.3 3.2 collective-permute-start
  180.8 15.1 %all-gather.20.cloned.1.call-done = bf16[1536,8,64]{0,2,1:T(8,128)(2,1)} async-done(((bf16[384,8,64]{0,2,1:T(8,128)(2,1)}), bf16[1536,8,64]{0,2,1:T(8,128)(2,1)}) %all-gather.20.cloned.1.call-update) | async-done | bytes 1572880 | tf_op jit(solution)/shard_map/all_gather | solution.py:116
  195.9 36.8 %conditional.1 = (f32[4,384]{1,0:T(4,128)}, f32[384,4,64]{0,2,1:T(8,128)}) conditional(s32[]{:T(128)} %bitcast.13, () %tuple.20, (bf16[1536,8,64]{0,2,1:T(8,128)(2,1)}, f32[1536,4]{0,1:T(4,128)}, s32[3,512]{1,0:T(4,128)S(1)}, s32[3,512]{1,0:T(4,128)S(1)}, s32[384]{0:T(512)}, /*index=5*/bf16[384,4,64]{0,2,1:T(8,128)(2,1)}, f32[384,4]{0,1:T(4,128)}) %tuple.21), branch_computations={%region_7.8_spmd, %region_8.13_spmd} | conditional | flops 215199744 | bytes 18206496 | solution.py:141
  199.3 33.4 %while.18 = (s32[]{:T(128)}, f32[4,384]{1,0:T(4,128)S(1)}, f32[4,384]{1,0:T(4,128)}, f32[384,4,64]{0,2,1:T(8,128)}, s32[384]{0:T(512)}, /*index=5*/s32[3,512]{1,...) while((s32[]{:T(128)}, f32[4,384]{1,0:T(4,128)S(1)}, ...), condition=%wide.region_12.12_spmd.clone, body=%wide.region_9.11_spmd.clone.sunk | while | flops 215196672 | bytes 11896481 | solution.py:136
  201.6 2.7 fusion.86
  204.9 1.6 fusion.88
  207.2 2.8 fusion.90
  212.2 2.7 fusion.86
  215.5 1.6 fusion.88
  218.5 2.9 fusion.90
  223.5 2.7 fusion.86
  226.9 1.6 fusion.88
  229.9 2.9 fusion.90
  234.9 44.1 %all-gather.12.cloned.1.call-done = bf16[2048,1024]{1,0:T(8,128)(2,1)} async-done(((bf16[512,1024]{1,0:T(8,128)(2,1)}), bf16[2048,1024]{1,0:T(8,128)(2,1)}) %all-gather.12.cloned.1.call-update) | async-done | bytes 4194320 | tf_op jit(solution)/shard_map/all_gather | solution.py:183
  279.0 5.3 %add_divide_fusion = f32[384,1024]{1,0:T(8,128)} fusion(bf16[384,2048]{1,0:T(8,128)(2,1)S(1)} %copy-done.1, bf16[2048,1024]{1,0:T(8,128)(2,1)} %all-gather.12.cloned.1.call-done), kind=kOutput, calls=%fused_computation.44 | convolution fusion | flops 1611792384 | bytes 7340032 | tf_op jit(solution)/shard_map/dot_general | solution.py:186
  284.2 2.7 reshape.258
  288.1 36.6 %all-gather.26.cloned.1.call-done = bf16[2,1024,512]{2,1,0:T(8,128)(2,1)} async-done(((bf16[2,256,512]{2,1,0:T(8,128)(2,1)}), bf16[2,1024,512]{2,1,0:T(8,128)(2,1)}) %all-gather.26.cloned.1.call-update) | async-done | bytes 2097168 | tf_op jit(solution)/shard_map/all_gather | solution.py:212
  324.7 20.2 %all-gather.24.cloned.1.call-done = bf16[384,2,1024]{2,0,1:T(8,128)(2,1)} async-done(((bf16[384,2,256]{2,0,1:T(8,128)(2,1)}), bf16[384,2,1024]{2,0,1:T(8,128)(2,1)}) %all-gather.24.cloned.1.call-update) | async-done | bytes 1572880 | tf_op jit(solution)/shard_map/all_gather | solution.py:217
  344.9 3.0 convolution_bitcast_fusion
  (134 shorter events, 44.8 us)
Async XLA Ops:
  6.5 26.7 %copy-start.11 = (f32[2048]{0:T(1024)S(1)}, f32[2048]{0:T(1024)}, u32[]{:S(2)}) copy-start(f32[2048]{0:T(1024)} %param.18) | copy-start | bytes 24580
  6.5 24.7 %all-gather.10.cloned.1.call-start = ((), (), s32[]{:S(2)}) async-start(), calls=%async_computation | async-start | bytes 1966080 | tf_op jit(solution)/shard_map/all_gather | solution.py:168
  7.3 53.6 %all-gather.16.cloned.1.call-start = ((), (), s32[]{:S(2)}) async-start(), calls=%async_computation.3 | async-start | bytes 1310720 | tf_op jit(solution)/shard_map/all_gather | solution.py:181
  8.0 81.8 %all-gather.18.cloned.1.call-start = ((), (), s32[]{:S(2)}) async-start(), calls=%async_computation.4 | async-start | bytes 1310720 | tf_op jit(solution)/shard_map/all_gather | solution.py:182
  8.7 142.4 %all-gather.22.cloned.1.call-start = ((), (), s32[]{:S(2)}) async-start(), calls=%async_computation.6 | async-start | bytes 1310720 | tf_op jit(solution)/shard_map/all_gather | solution.py:180
  9.3 148.3 %all-gather.14.cloned.1.call-start = ((), (), s32[]{:S(2)}) async-start(), calls=%async_computation.2 | async-start | bytes 1310720 | tf_op jit(solution)/shard_map/all_gather | solution.py:177
  9.9 186.0 %all-gather.20.cloned.1.call-start = ((), (), s32[]{:S(2)}) async-start(), calls=%async_computation.5 | async-start | bytes 1966080 | tf_op jit(solution)/shard_map/all_gather | solution.py:116
  31.3 1.9 copy-start.2
  33.7 137.0 %copy-start = (bf16[384,2048]{1,0:T(8,128)(2,1)}, bf16[384,2048]{1,0:T(8,128)(2,1)S(1)}, u32[]{:S(2)}) copy-start(bf16[384,2048]{1,0:T(8,128)(2,1)S(1)} %fusion.27) | copy-start | bytes 4718596
  63.0 29.7 %copy-start.5 = (bf16[512,2,512]{2,1,0:T(2,128)(2,1)S(1)}, bf16[512,2,512]{2,1,0:T(2,128)(2,1)}, u32[]{:S(2)}) copy-start(bf16[512,2,512]{2,1,0:T(2,128)(2,1)} %param.28) | copy-start | bytes 3145732
  92.6 186.3 %all-gather.12.cloned.1.call-start = ((), (), s32[]{:S(2)}) async-start(), calls=%async_computation.1 | async-start | bytes 5242880 | tf_op jit(solution)/shard_map/all_gather | solution.py:183
  92.7 19.1 %copy-start.9 = (bf16[512,128]{1,0:T(8,128)(2,1)S(1)}, bf16[512,128]{1,0:T(8,128)(2,1)}, u32[]{:S(2)}) copy-start(bf16[512,128]{1,0:T(8,128)(2,1)} %param.21) | copy-start | bytes 393220
  94.0 36.4 %copy-start.14 = (f32[4]{0:T(128)S(1)}, f32[4]{0:T(128)}, u32[]{:S(2)}) copy-start(f32[4]{0:T(128)} %param.23) | copy-start | bytes 52
  94.0 36.5 %copy-start.10 = (bf16[512,128]{1,0:T(8,128)(2,1)S(1)}, bf16[512,128]{1,0:T(8,128)(2,1)}, u32[]{:S(2)}) copy-start(bf16[512,128]{1,0:T(8,128)(2,1)} %param.22) | copy-start | bytes 393220
  94.0 230.7 %all-gather.26.cloned.1.call-start = ((), (), s32[]{:S(2)}) async-start(), calls=%async_computation.8 | async-start | bytes 2621440 | tf_op jit(solution)/shard_map/all_gather | solution.py:212
  94.8 250.2 %all-gather.24.cloned.1.call-start = ((), (), s32[]{:S(2)}) async-start(), calls=%async_computation.7 | async-start | bytes 1966080 | tf_op jit(solution)/shard_map/all_gather | solution.py:217
  166.5 0.6 copy-start.6
  166.5 8.1 %copy-start.4 = (f32[6,64,2,2]{3,2,1,0:T(2,128)S(1)}, f32[6,64,2,2]{3,2,1,0:T(2,128)}, u32[]{:S(2)}) copy-start(f32[6,64,2,2]{3,2,1,0:T(2,128)} %copy.39) | copy-start | bytes 18436
  166.5 8.1 %copy-start.12 = (f32[64]{0:T(128)S(1)}, f32[64]{0:T(128)}, u32[]{:S(2)}) copy-start(f32[64]{0:T(128)} %get-tuple-element.197) | copy-start | bytes 772
  167.1 9.5 %collective-permute-start.1 = (bf16[128,2,64]{0,2,1:T(8,128)(2,1)}, bf16[128,2,64]{0,2,1:T(8,128)(2,1)S(1)}, u32[]{:S(2)}, u32[]{:S(2)}) collective-permute-start(bf16[128,2,64]{0,2,1:T(8,128)(2,1)} %slice.68), channel_id=1, source_target_pairs={{0,4},{4,8},{8,12},{1,5},{5,9},{9,13},{2,6},{6,10},{10,14},{3,7},{... | collective-permute-start | bytes 98312 | tf_op jit(solution)/shard_map/ppermute | solution.py:16
  171.3 4.4 %copy-start.3 = (f32[384,256]{0,1:T(8,128)S(1)}, f32[384,256]{0,1:T(8,128)}, u32[]{:S(2)}) copy-start(f32[384,256]{0,1:T(8,128)} %get-tuple-element.204) | copy-start | bytes 1179652
  171.3 4.4 %copy-start.13 = (f32[64]{0:T(128)S(1)}, f32[64]{0:T(128)}, u32[]{:S(2)}) copy-start(f32[64]{0:T(128)} %get-tuple-element.199) | copy-start | bytes 772
  171.3 5.9 %collective-permute-start = (bf16[128,2,64]{0,2,1:T(8,128)(2,1)S(1)}, bf16[128,2,64]{0,2,1:T(8,128)(2,1)S(1)}, u32[]{:S(2)}, u32[]{:S(2)}) collective-permute-start(bf16[128,2,64]{0,2,1:T(8,128)(2,1)S(1)} %bitcast.167), channel_id=1, source_target_pairs={{0,4},{4,8},{8,12},{1,5},{5,9},{9,13},{2,6},{6,10},{10,14},{3,7},{... | collective-permute-start | bytes 98312 | tf_op jit(solution)/shard_map/ppermute | solution.py:16
  174.6 2.1 copy-start.7
  177.0 0.9 copy-start.8
  232.7 46.2 %copy-start.1 = (bf16[384,2048]{1,0:T(8,128)(2,1)S(1)}, bf16[384,2048]{1,0:T(8,128)(2,1)}, u32[]{:S(2)}) copy-start(bf16[384,2048]{1,0:T(8,128)(2,1)} %copy-done) | copy-start | bytes 4718596
Sparse Core Ops, SparseCore 0:
  8.9 22.3 all-gather.9
  32.8 27.9 all-gather.15
  62.4 27.3 all-gather.17
  91.3 33.3 all-gather.21
  126.1 31.5 all-gather.13
  159.0 36.8 all-gather.19
  197.5 81.4 all-gather.11
  280.5 44.1 all-gather.25
  326.3 18.6 all-gather.23
